TPU v7x, 32 devices: a whole 2x2x4 slice. The times are simulated.
32 devices in a mesh: ep: 8 (over z, x), tp: 4 (over y, core).
Axes of the slice: x: 2, y: 2, z: 4, core: 2. Of those that a mesh axis runs over, the one named last changes fastest.
Arguments:
- mixer_tokens: bfloat16 [1536, 2048], P('ep'), may hold values from -6 to 6
- mixer_gain: float32 [2048], replicated, may hold values from 0.1 to 1.9
- query_weight: bfloat16 [1024, 2048], P('tp'), may hold values from -1 to 1
- key_weight: bfloat16 [1024, 2048], P('tp'), may hold values from -1 to 1
- value_weight: bfloat16 [1024, 2048], P('tp'), may hold values from -0.125 to 0.125
- forget_weight: bfloat16 [2048, 16], P(None, 'tp'), may hold values from -0.125 to 0.125
- forget_bias: float32 [8, 16], P('ep', 'tp'), may hold values from 2.98 to 10.4
- output_weight: bfloat16 [1024, 2048], P(None, 'tp'), may hold values from -0.1875 to 0.1875
- expert_tokens: bfloat16 [1024, 2048], P('ep'), may hold values from -6 to 6
- expert_gain: float32 [2048], replicated, may hold values from 0.1 to 1.9
- routes: int32 [1024, 2], P('ep'), may hold values from 0 to 7, all different within a row; in each aligned block of 128 rows (0 to 127, 128 to 255, ...) at most 64 rows name the same one
- route_weights: float32 [1024, 2], P('ep'), may hold values from 0.2 to 1
- gate_weight: bfloat16 [8, 3584, 2048], P('ep', 'tp'), may hold values from -0.125 to 0.125
- up_weight: bfloat16 [8, 3584, 2048], P('ep', 'tp'), may hold values from -0.125 to 0.125
- down_weight: bfloat16 [8, 3584, 2048], P('ep', 'tp'), may hold values from -0.09375 to 0.09375
Outputs:
- mixer_output: bfloat16 [1536, 2048], P('ep', 'tp')
- expert_output: bfloat16 [1024, 2048], P('ep', 'tp')
Inputs may be any that keep to these rules, and one draw needn't show every extreme that they name: `routes`: within the tokens of one index of ep (aligned blocks of 128 rows) no expert is named more than 64 times, a bound that some block reaches; the 2 experts of a token differ.
All inputs are finite; a program needn't handle non-finite values.
Results may differ from a plain program's by a relative error of at most 0.019.
Values may be sent and summed in bfloat16 or wider, within the bound.
A program may use at most 128 MiB of HBM per device.

v0:
```python
import jax
import jax.numpy as jnp
from jax import lax
from jax.sharding import PartitionSpec as P

HD = 64


MEAN_FLOOR = 0.1
HEAD_FLOOR = 1.0
START_MAX = -1e30


def normed_rows(inputs, gain):
    values = inputs.astype(jnp.float32)
    square = jnp.mean(values * values, axis=-1, keepdims=True)
    return (values * lax.rsqrt(jnp.maximum(square, MEAN_FLOOR)) * gain).astype(jnp.bfloat16)


def by_rows(left, weight):
    return lax.dot_general(
        left, weight, (((1,), (1,)), ((), ())), preferred_element_type=jnp.float32
    )


def on_device(
    mixer_tokens,
    mixer_gain,
    query_weight,
    key_weight,
    value_weight,
    forget_weight,
    forget_bias,
    output_weight,
    expert_tokens,
    expert_gain,
    routes,
    route_weights,
    gate_weight,
    up_weight,
    down_weight,
):
    row_count = mixer_tokens.shape[0]
    feature_count = mixer_tokens.shape[1]
    local_heads = forget_weight.shape[1]
    normed = normed_rows(mixer_tokens, mixer_gain)
    queries = by_rows(normed, query_weight).astype(jnp.bfloat16)
    key_rows = by_rows(normed, key_weight).astype(jnp.bfloat16)
    value_rows = by_rows(normed, value_weight).astype(jnp.bfloat16)
    pre_gate = jnp.dot(normed, forget_weight, preferred_element_type=jnp.float32) + forget_bias
    log_gates = jax.nn.log_sigmoid(pre_gate)
    all_gates = lax.all_gather(log_gates, "ep", axis=0, tiled=True)
    cumulative = jnp.cumsum(all_gates, axis=0)
    offset = lax.axis_index("ep") * row_count
    query_cum = lax.dynamic_slice_in_dim(cumulative, offset, row_count, 0)
    head_query = queries.reshape(row_count, local_heads, HD)
    query_pos = offset + jnp.arange(row_count, dtype=jnp.int32)
    initial = (
        jnp.full((local_heads, row_count), START_MAX, jnp.float32),
        jnp.zeros((row_count, local_heads, HD), jnp.float32),
    )
    pieces = (
        lax.all_gather(key_rows, "ep", axis=0, tiled=True),
        lax.all_gather(value_rows, "ep", axis=0, tiled=True),
    )

    def compute(current):
        running, accumulated = current
        piece_keys, piece_values = pieces
        key_count = piece_keys.shape[0]
        scores = jnp.einsum(
            "qhd,khd->hqk",
            head_query,
            piece_keys.reshape(key_count, local_heads, HD),
            preferred_element_type=jnp.float32,
        ) * HD ** (-0.5)
        scores = scores + query_cum.T[:, :, None] - cumulative.T[:, None, :]
        key_pos = jnp.arange(key_count, dtype=jnp.int32)
        scores = jnp.where(key_pos[None, None, :] <= query_pos[None, :, None], scores, -jnp.inf)
        new_max = jnp.maximum(running, jnp.max(scores, axis=-1))
        weights = jnp.exp(scores - new_max[:, :, None]).astype(jnp.bfloat16)
        update = jnp.einsum(
            "hqk,khd->qhd",
            weights,
            piece_values.reshape(key_count, local_heads, HD),
            preferred_element_type=jnp.float32,
        )
        factor = jnp.exp(running - new_max).T[:, :, None]
        return (new_max, accumulated * factor + update)

    running, accumulated = lax.cond(
        jnp.int32(0) < offset + row_count, compute, lambda current: current, initial
    )
    rescale = lax.rsqrt(jnp.mean(accumulated * accumulated, axis=-1, keepdims=True) + HEAD_FLOOR)
    head_out = (accumulated * rescale).reshape(row_count, local_heads * HD).astype(jnp.bfloat16)
    mixer_output = jnp.dot(
        lax.all_gather(head_out, "tp", axis=1, tiled=True),
        output_weight,
        preferred_element_type=jnp.float32,
    ).astype(jnp.bfloat16)
    expert_normed = normed_rows(expert_tokens, expert_gain)
    token_count, top_count = routes.shape
    experts = lax.axis_size("ep")
    capacity = 2 * top_count * token_count // experts
    flat_routes = routes.reshape(-1)
    onehot = (flat_routes[:, None] == jnp.arange(experts, dtype=jnp.int32)[None, :]).astype(
        jnp.int32
    )
    slot_rank = jnp.sum((jnp.cumsum(onehot, axis=0) - 1) * onehot, axis=1)
    slot_index = flat_routes * capacity + slot_rank
    slot_owner = jnp.full((experts * capacity,), token_count, jnp.int32)
    slot_owner = slot_owner.at[slot_index].set(
        jnp.arange(token_count * top_count, dtype=jnp.int32) // top_count
    )
    padded = jnp.concatenate([expert_normed, jnp.zeros((1, feature_count), jnp.bfloat16)], axis=0)
    outgoing = padded[slot_owner].reshape(experts, capacity, feature_count)
    column_count = feature_count // lax.axis_size("tp")
    column_start = lax.axis_index("tp") * column_count
    slices = lax.dynamic_slice_in_dim(outgoing, column_start, column_count, 2)
    slots = lax.all_gather(
        lax.all_to_all(slices, "ep", split_axis=0, concat_axis=0, tiled=True),
        "tp",
        axis=2,
        tiled=True,
    )
    sources, slot_count, _ = slots.shape
    flat_rows = slots.reshape(sources * slot_count, feature_count)
    gate_act = by_rows(flat_rows, gate_weight[0])
    up_act = by_rows(flat_rows, up_weight[0])
    hidden = (jax.nn.silu(gate_act) * up_act).astype(jnp.bfloat16)
    partial_value = jnp.dot(hidden, down_weight[0], preferred_element_type=jnp.float32)
    partial_value = partial_value.reshape(sources, slot_count, feature_count)
    summed = lax.psum_scatter(
        partial_value.astype(jnp.bfloat16), "tp", scatter_dimension=2, tiled=True
    )
    returned = lax.all_to_all(summed, "ep", split_axis=0, concat_axis=0, tiled=True)
    gathered = returned.reshape(experts * capacity, returned.shape[2])[slot_index]
    weighted = gathered.astype(jnp.float32) * route_weights.reshape(-1)[:, None]
    expert_output = jnp.sum(weighted.reshape(token_count, top_count, returned.shape[2]), axis=1)
    return (mixer_output, expert_output.astype(jnp.bfloat16))


def solution(mesh):
    in_specs = (
        P("ep", None),
        P(),
        P("tp", None),
        P("tp", None),
        P("tp", None),
        P(None, "tp"),
        P("ep", "tp"),
        P(None, "tp"),
        P("ep", None),
        P(),
        P("ep", None),
        P("ep", None),
        P("ep", "tp", None),
        P("ep", "tp", None),
        P("ep", "tp", None),
    )
    out_specs = (P("ep", "tp"), P("ep", "tp"))
    return jax.shard_map(
        on_device, mesh=mesh, in_specs=in_specs, out_specs=out_specs, check_vma=False
    )
```

profile of v0, /device:TPU:0, one launch (start us, length us, event | category | flops | bytes accessed | tf_op | source)
XLA Modules:
  0.0 207.6 jit_solution(10816448384278790010)
XLA Ops:
  10.3 1.4 scatter_custom_fusion
  11.7 1.2 fusion.19
  12.9 1.2 fusion.21
  14.2 3.3 %gather_fusion = bf16[512,2048]{1,0:T(8,128)(2,1)} fusion(bf16[129,2048]{1,0:T(8,128)(2,1)S(1)} %concatenate.3, s32[1024]{0:T(1024)S(1)} %pad_clamp_fusion.1), kind=kCustom, calls=%fused_computation | custom fusion | bytes 4196352 | tf_op jit(solution)/shard_map/gather | solution.py:116
  17.6 1.1 constant_dynamic-slice_fusion
  18.7 21.7 %all_to_all.10 = bf16[8,64,512]{2,1,0:T(8,128)(2,1)} all-to-all(bf16[8,64,512]{2,1,0:T(8,128)(2,1)S(1)} %constant_dynamic-slice_fusion), channel_id=1, replica_groups=mesh['ep'=8,'tp'=4] {'ep'}, dimensions={0} | all-to-all | bytes 1048576 | tf_op jit(solution)/shard_map/all_to_all | solution.py:121
  40.4 21.7 %all-gather.3.cloned.1.call-done = bf16[8,64,2048]{2,1,0:T(8,128)(2,1)} async-done(((bf16[8,64,512]{2,1,0:T(8,128)(2,1)}), bf16[8,64,2048]{2,1,0:T(8,128)(2,1)}) %all-gather.3.cloned.1.call-update) | async-done | bytes 2097168 | tf_op jit(solution)/shard_map/all_gather | solution.py:120
  62.2 5.2 %fusion.8 = f32[512,896]{1,0:T(8,128)S(1)} fusion(bf16[512,2048]{1,0:T(8,128)(2,1)} %bitcast.89, bf16[1,896,2048]{2,1,0:T(8,128)(2,1)} %param.29), kind=kOutput, calls=%fused_computation.18 | convolution fusion | flops 1879048192 | bytes 7602176 | tf_op jit(solution)/shard_map/dot_general | solution.py:21
  67.4 2.4 %multiply_convert_fusion = bf16[512,896]{1,0:T(8,128)(2,1)S(1)} fusion(f32[512,896]{1,0:T(8,128)S(1)} %fusion.8, bf16[512,2048]{1,0:T(8,128)(2,1)S(1)} %bitcast.90, bf16[1,896,2048]{2,1,0:T(8,128)(2,1)S(1)} %copy-done.3), kind=kOutput, calls=%fused_computation.23 | convolution fusion | flops 1881800704 | bytes 8519680 | tf_op jit(solution)/shard_map/dot_general | solution.py:21
  69.8 3.7 %fusion.10 = bf16[8,64,2048]{2,1,0:T(8,128)(2,1)} fusion(bf16[8,64,896]{2,1,0:T(8,128)(2,1)S(1)} %bitcast.92, bf16[1,896,2048]{2,1,0:T(8,128)(2,1)S(1)} %copy-done.4), kind=kOutput, calls=%fused_computation.20 | convolution fusion | flops 1880096768 | bytes 6684672 | tf_op jit(solution)/shard_map/dot_general | solution.py:131
  73.5 1.1 copy-done.1
  75.3 30.7 %all-gather = f32[8,192,4]{1,2,0:T(4,128)S(1)} all-gather(f32[1,192,4]{1,2,0:T(4,128)S(1)} %fusion.25), channel_id=1, replica_groups=mesh['ep'=8,'tp'=4] {'ep'}, dimensions={0}, use_global_device_ids=true | all-gather | bytes 27648 | tf_op jit(solution)/shard_map/all_gather | solution.py:52
  106.1 1.2 reduce-window.14
  110.0 32.1 %all_gather.15 = bf16[1536,256]{1,0:T(8,128)(2,1)S(1)} all-gather(bf16[192,256]{1,0:T(8,128)(2,1)S(1)} %convolution_convert_fusion.2), channel_id=1, replica_groups=mesh['ep'=8,'tp'=4] {'ep'}, dimensions={0}, use_global_device_ids=true | all-gather | bytes 884736 | tf_op jit(solution)/shard_map/all_gather | solution.py:63
  142.1 32.0 %all_gather.17 = bf16[1536,256]{1,0:T(8,128)(2,1)S(1)} all-gather(bf16[192,256]{1,0:T(8,128)(2,1)S(1)} %convolution_convert_fusion.1), channel_id=1, replica_groups=mesh['ep'=8,'tp'=4] {'ep'}, dimensions={0}, use_global_device_ids=true | all-gather | bytes 884736 | tf_op jit(solution)/shard_map/all_gather | solution.py:64
  174.1 6.2 %all-to-all-start.1 = ((bf16[8,64,512]{2,1,0:T(8,128)(2,1)}), bf16[8,64,512]{2,1,0:T(8,128)(2,1)S(1)}, u32[]{:S(2)}, u32[]{:S(2)}) async-start(bf16[8,64,512]{2,1,0:T(8,128)(2,1)} %reduce-scatter.2.cloned.1.call-done), calls=%async_computation.2 | async-start | bytes 1048576 | tf_op jit(solution)/shard_map/all_to_all | solution.py:136
  180.5 9.7 %conditional.1 = (f32[192,4,64]{0,2,1:T(8,128)S(1)}, f32[192,4,1]{0,1,2:T(4,128)S(1)}) conditional(s32[]{:T(128)} %convert_element_type.57, () %tuple.18, (s32[]{:T(128)}, s32[192]{0:T(256)S(1)}, bf16[192,256]{1,0:T(8,128)(2,1)S(1)}, bf16[1536,256]{1,0:T(8,128)(2,1)S(1)}, f32[192,4]{0,1:T(4,128)S(1)}, /*index=5*/f32[1536,4]{0,1:T(4,128)S(1)}, ...), branch_computations={%region_3.4_spmd, %region_4.7_spmd} | conditional | flops 310690752 | bytes 15288596 | solution.py:91
  180.5 1.2 copy.33
  182.1 4.6 %fusion.32 = (f32[4,192]{1,0:T(4,128)S(1)}, f32[4,192,1536]{2,1,0:T(8,128)}) fusion(f32[4,1536]{1,0:T(4,128)S(1)} %bitcast.82, f32[4,192]{1,0:T(4,128)S(1)} %bitcast.87, bf16[192,4,64]{0,2,1:T(8,128)(2,1)S(1)} %bitcast.78, bf16[1536,4,64]{0,2,1:T(8,128)(2,1)} %bitcast.76, pred[192,1536]{1,0:T(8,128)(4,1)S(1)} %iota_compare_fusion), kind=kOutput, calls=%fused_computation.68 | convolution fusion | flops 156892416 | bytes 5928960 | tf_op jit(solution)/shard_map/cond/branch_1_fun/qhd,khd->hqk/dot_general | solution.py:71
  186.9 3.3 %multiply_reduce_fusion = (f32[192,4]{0,1:T(4,128)S(1)}, f32[192,4,64]{0,2,1:T(8,128)S(1)}) fusion(bf16[1536,4,64]{0,2,1:T(8,128)(2,1)S(1)} %bitcast.75, f32[4,192,1536]{2,1,0:T(8,128)} %get-tuple-element.56, f32[4,192]{1,0:T(4,128)S(1)} %get-tuple-element.54, f32[192,4]{0,1:T(4,128)S(1)} %get-tuple-element.53), kind=kOutput, calls=%fused_computation.10 | convolution fusion | flops 153500928 | bytes 5710848 | tf_op jit(solution)/shard_map/cond/branch_1_fun/hqk,khd->qhd/dot_general | solution.py:82
  190.3 6.5 %all_gather.18 = bf16[192,1024]{0,1:T(8,128)(2,1)S(1)} all-gather(bf16[192,256]{0,1:T(8,128)(2,1)S(1)} %bitcast.77), channel_id=1, replica_groups=mesh['ep'=8,'tp'=4] {'tp'}, dimensions={1}, use_global_device_ids=true | all-gather | bytes 491520 | tf_op jit(solution)/shard_map/all_gather | solution.py:97
  196.8 1.1 convolution_convert_fusion
  197.9 1.2 gather_fusion.1
  199.4 1.4 multiply_reduce_fusion.1
  (73 shorter events, 7.9 us)
Async XLA Ops:
  7.2 189.7 %copy-start = (bf16[1024,512]{1,0:T(8,128)(2,1)S(1)}, bf16[1024,512]{1,0:T(8,128)(2,1)}, u32[]{:S(2)}) copy-start(bf16[1024,512]{1,0:T(8,128)(2,1)} %param.24) | copy-start | bytes 3145732
  7.2 55.0 %all-gather.3.cloned.1.call-start = ((), (), s32[]{:S(2)}) async-start(), calls=%async_computation.3 | async-start | bytes 2621440 | tf_op jit(solution)/shard_map/all_gather | solution.py:120
  40.4 133.7 %reduce-scatter.2.cloned.1.call-start = ((), (), s32[]{:S(2)}) async-start(), calls=%async_computation.4 | async-start | bytes 2621440 | tf_op jit(solution)/shard_map/reduce_scatter | solution.py:133
  62.1 5.2 %copy-start.3 = (bf16[1,896,2048]{2,1,0:T(8,128)(2,1)S(1)}, bf16[1,896,2048]{2,1,0:T(8,128)(2,1)}, u32[]{:S(2)}) copy-start(bf16[1,896,2048]{2,1,0:T(8,128)(2,1)} %param.30) | copy-start | bytes 11010052
  62.2 5.2 %copy-start.5 = (bf16[8,64,2048]{2,1,0:T(8,128)(2,1)S(1)}, bf16[8,64,2048]{2,1,0:T(8,128)(2,1)}, u32[]{:S(2)}) copy-start(bf16[8,64,2048]{2,1,0:T(8,128)(2,1)} %all-gather.3.cloned.1.call-done) | copy-start | bytes 6291460
  67.4 2.4 %copy-start.4 = (bf16[1,896,2048]{2,1,0:T(8,128)(2,1)S(1)}, bf16[1,896,2048]{2,1,0:T(8,128)(2,1)}, u32[]{:S(2)}) copy-start(bf16[1,896,2048]{2,1,0:T(8,128)(2,1)} %param.31) | copy-start | bytes 11010052
  73.5 1.1 copy-start.1
  73.5 1.4 copy-start.9
  73.5 1.4 copy-start.10
  73.5 1.4 copy-start.11
  73.5 34.2 %copy-start.6 = (bf16[256,2048]{1,0:T(8,128)(2,1)S(1)}, bf16[256,2048]{1,0:T(8,128)(2,1)}, u32[]{:S(2)}) copy-start(bf16[256,2048]{1,0:T(8,128)(2,1)} %param.20) | copy-start | bytes 3145732
  107.7 1.2 copy-start.7
  107.8 1.7 copy-start.8
  109.5 70.9 %copy-start.2 = (f32[128,2]{0,1:T(2,128)S(1)}, f32[128,2]{0,1:T(2,128)}, u32[]{:S(2)}) copy-start(f32[128,2]{0,1:T(2,128)} %param.28) | copy-start | bytes 3076
  174.1 23.8 %all-to-all-start.1 = ((bf16[8,64,512]{2,1,0:T(8,128)(2,1)}), bf16[8,64,512]{2,1,0:T(8,128)(2,1)S(1)}, u32[]{:S(2)}, u32[]{:S(2)}) async-start(bf16[8,64,512]{2,1,0:T(8,128)(2,1)} %reduce-scatter.2.cloned.1.call-done), calls=%async_computation.2 | async-start | bytes 1048576 | tf_op jit(solution)/shard_map/all_to_all | solution.py:136
Sparse Core Ops, SparseCore 0:
  40.5 21.5 all-gather.2
  73.7 31.1 reduce-scatter.1
where the time goes:
time: 208 us
  blocking collectives  123 us (59%)
  matrix products  22.2 us (11%)
  waiting for transfers between devices  21.7 us (10%)
  between operations  14.3 us (7%)
  local copies, waits for them, and re-layouts  12.8 us (6%)
  other arithmetic  7.21 us (3%)
  starting transfers between devices  6.33 us (3%)
    all_gather x1, blocking collectives, on_device(): lax.all_gather(key_rows, 'ep', axis=0, tiled=True)  32.1 us
    all_gather x1, blocking collectives, on_device(): lax.all_gather(value_rows, 'ep', axis=0, tiled=True)  32 us
    all_gather x1, blocking collectives, on_device(): all_gates = lax.all_gather(log_gates, 'ep', axis=0, tiled=True)  30.7 us
    all_to_all x1, blocking collectives, on_device(): lax.all_to_all(slices, 'ep', split_axis=0, concat_axis=0, tiled=True)  21.7 us
    all_gather x1, waiting for transfers between devices, on_device(): lax.all_gather(lax.all_to_all(slices, 'ep', split_axis=0, concat_axis=0,...  21.7 us
    dot_general x5, matrix products, by_rows(): lax.dot_general(left, weight, (((1,), (1,)), ((), ())), preferred_element...  9.14 us
    all_gather x1, blocking collectives, on_device(): lax.all_gather(head_out, 'tp', axis=1, tiled=True)  6.5 us
    all_to_all x1, starting transfers between devices, on_device(): lax.all_to_all(summed, 'ep', split_axis=0, concat_axis=0, tiled=True)  6.25 us
  transfers between devices with their start and end apart: 3, of which 1 were waited for; matrix products, arithmetic and copies ran while one was open for 7% of the time, Pallas kernels for 0%

commit v1 on v0

v1 whole, which is shorter than its diff:
```python
import functools

import jax
import jax.numpy as jnp
from jax import lax
from jax.experimental import pallas as pl
from jax.experimental.pallas import tpu as pltpu
from jax.sharding import PartitionSpec as P

HD = 64
MEAN_FLOOR = 0.1
HEAD_FLOOR = 1.0
MESH = pl.DeviceIdType.MESH
VM = pl.BlockSpec(memory_space=pltpu.VMEM)
DMA = pltpu.SemaphoreType.DMA


def normed_rows(inputs, gain):
    values = inputs.astype(jnp.float32)
    square = jnp.mean(values * values, axis=-1, keepdims=True)
    return (values * lax.rsqrt(jnp.maximum(square, MEAN_FLOOR)) * gain).astype(jnp.bfloat16)


def by_rows(left, weight):
    return lax.dot_general(
        left, weight, (((1,), (1,)), ((), ())), preferred_element_type=jnp.float32
    )


class Place:
    def __init__(self, n_ep, n_tp):
        self.n_ep, self.n_tp, self.ny = n_ep, n_tp, n_tp // 2
        self.e = lax.axis_index("ep")
        self.t = lax.axis_index("tp")
        self.y, self.c = self.t // 2, self.t % 2
        self.partner = self.y * 2 + (1 - self.c)

    def ep(self, k):
        return (self.e + k) % self.n_ep

    def y_at(self, off):
        return (self.y + self.ny + off) % self.ny

    def chip(self, off):
        return self.y_at(off) * 2 + self.c

    def barrier(self):
        sem = pltpu.get_barrier_semaphore()
        for k in range(1, self.n_ep):
            pl.semaphore_signal(
                sem, inc=1, device_id={"ep": self.ep(k), "tp": self.t}, device_id_type=MESH
            )
        for off in range(1, self.ny):
            pl.semaphore_signal(
                sem, inc=1, device_id={"ep": self.e, "tp": self.chip(off)}, device_id_type=MESH
            )
        pl.semaphore_signal(
            sem, inc=1, device_id={"ep": self.e, "tp": self.partner}, device_id_type=MESH
        )
        pl.semaphore_wait(sem, self.n_ep - 1 + self.ny - 1 + 1)


def remote(src, dst, send, recv, e, t):
    return pltpu.make_async_remote_copy(
        src_ref=src,
        dst_ref=dst,
        send_sem=send,
        recv_sem=recv,
        device_id={"ep": e, "tp": t},
        device_id_type=MESH,
    )


class Exchange:
    def __init__(self, place, send, land, sems):
        self.p, self.send, self.land = place, send, land
        self.ssem, self.rsem = sems

    def copy(self, k):
        p = self.p
        d = p.ep(k)
        return remote(
            self.send(d), self.land(p.e), self.ssem.at[d], self.rsem.at[p.e], d, p.t
        )

    def arrival(self, k):
        p = self.p
        s = p.ep(k)
        return remote(self.send(s), self.land(s), self.ssem.at[s], self.rsem.at[s], s, p.t)

    def own(self):
        p = self.p
        return pltpu.make_async_copy(self.send(p.e), self.land(p.e), self.rsem.at[p.e])

    def start(self):
        for k in range(1, self.p.n_ep):
            self.copy(k).start()
        self.own().start()

    def wait_arrival(self, k):
        if k == 0:
            self.own().wait()
        else:
            self.arrival(k).wait_recv()

    def wait_sent(self):
        for k in range(1, self.p.n_ep):
            self.copy(k).wait_send()


class Spread:
    def __init__(self, place, land, sems):
        self.p, self.land = place, land
        self.ys, self.yr, self.ps, self.pr = sems

    def y_copy(self, off, s):
        p = self.p
        block = self.land(p.t, s)
        return remote(
            block, block, self.ys.at[off - 1, s], self.yr.at[off - 1, s], p.e, p.chip(off)
        )

    def y_arrival(self, off, s):
        p = self.p
        block = self.land(p.chip(-off), s)
        return remote(
            block, block, self.ys.at[off - 1, s], self.yr.at[off - 1, s], p.e, p.chip(-off)
        )

    def p_copy(self, off, s):
        p = self.p
        block = self.land(p.chip(-off), s)
        return remote(block, block, self.ps.at[off, s], self.pr.at[off, s], p.e, p.partner)

    def p_arrival(self, off, s):
        p = self.p
        block = self.land(p.y_at(-off) * 2 + (1 - p.c), s)
        return remote(block, block, self.ps.at[off, s], self.pr.at[off, s], p.e, p.partner)

    def first(self, s):
        for off in range(1, self.p.ny):
            self.y_copy(off, s).start()
        self.p_copy(0, s).start()

    def relay(self, s):
        for off in range(1, self.p.ny):
            self.y_arrival(off, s).wait_recv()
            self.p_copy(off, s).start()

    def finish(self, s):
        for off in range(self.p.ny):
            self.p_arrival(off, s).wait_recv()
            self.p_copy(off, s).wait_send()
        for off in range(1, self.p.ny):
            self.y_copy(off, s).wait_send()


def spread_sems(n_ep, n_tp):
    ny = n_tp // 2
    far = max(ny - 1, 1)
    return [DMA((far, n_ep)), DMA((far, n_ep)), DMA((ny, n_ep)), DMA((ny, n_ep))]


def outward_kernel(
    n_ep, n_tp, slots, message, gates, out, message_out, gates_out,
    s0, s1, m0, m1, g0, g1, ys, yr, ps, pr,
):
    p = Place(n_ep, n_tp)
    width = slots.shape[2]

    def land(t, s):
        return out.at[s, :, pl.ds(pl.multiple_of(t * width, width), width)]

    p.barrier()
    slot_move = Exchange(p, lambda d: slots.at[d], lambda s: land(p.t, s), (s0, s1))
    gate_move = Exchange(p, lambda d: gates.at[d], lambda s: gates_out.at[s], (g0, g1))
    message_move = Exchange(p, lambda d: message.at[d], lambda s: message_out.at[s], (m0, m1))
    spread = Spread(p, land, (ys, yr, ps, pr))
    slot_move.start()
    gate_move.start()
    message_move.start()
    for k in range(n_ep):
        slot_move.wait_arrival(k)
        spread.first(p.ep(k))
    for k in range(n_ep):
        spread.relay(p.ep(k))
    for k in range(n_ep):
        gate_move.wait_arrival(k)
        message_move.wait_arrival(k)
        spread.finish(p.ep(k))
    slot_move.wait_sent()
    gate_move.wait_sent()
    message_move.wait_sent()


def homeward_kernel(
    n_ep, n_tp, partial, heads, ret, heads_all,
    pair, mine, out_y, in_y, final,
    h0, h1, a0, a1, r0, r1, q0, q1, ys, yr, ps, pr,
):
    p = Place(n_ep, n_tp)
    ny = p.ny
    width = ret.shape[2]

    def cols(t):
        return pl.ds(pl.multiple_of(t * width, width), width)

    def land(t, s):
        return heads_all.at[t, s]

    p.barrier()
    head_move = Exchange(p, lambda d: heads.at[d], lambda s: land(p.t, s), (h0, h1))
    spread = Spread(p, land, (ys, yr, ps, pr))
    head_move.start()

    def pair_copy(s, off):
        src = partial.at[s, :, cols(p.y_at(off) * 2 + (1 - p.c))]
        return remote(src, pair.at[s, off], r0.at[s, off], r1.at[s, off], p.e, p.partner)

    def y_copy(s, off, to):
        return remote(
            out_y.at[s, off - 1], in_y.at[s, off - 1],
            q0.at[s, off - 1], q1.at[s, off - 1], p.e, p.chip(to),
        )

    def final_copy(k):
        d = p.ep(k)
        return remote(final.at[d], ret.at[p.e], a0.at[d], a1.at[p.e], d, p.t)

    order = list(range(1, n_ep)) + [0]
    for k in order:
        for off in range(ny):
            pair_copy(p.ep(k), off).start()
    for k in order:
        s = p.ep(k)
        for off in [*range(1, ny), 0]:
            pair_copy(s, off).wait_recv()
            both = partial[s, :, cols(p.chip(off))].astype(jnp.float32) + pair[s, off].astype(
                jnp.float32
            )
            if off == 0:
                mine[s] = both
            else:
                out_y[s, off - 1] = both.astype(jnp.bfloat16)
                y_copy(s, off, off).start()
    for k in range(n_ep):
        head_move.wait_arrival(k)
        spread.first(p.ep(k))
    for k in order:
        s = p.ep(k)
        total = mine[s]
        for off in range(1, ny):
            y_copy(s, off, -off).wait_recv()
            total = total + in_y[s, off - 1].astype(jnp.float32)
        if k == 0:
            ret[s] = total.astype(jnp.bfloat16)
        else:
            final[s] = total.astype(jnp.bfloat16)
            final_copy(k).start()
    for k in range(n_ep):
        spread.relay(p.ep(k))
    for k in range(n_ep):
        spread.finish(p.ep(k))
    for k in range(n_ep):
        s = p.ep(k)
        for off in range(ny):
            pair_copy(s, off).wait_send()
        for off in range(1, ny):
            y_copy(s, off, off).wait_send()
    for k in range(1, n_ep):
        s = p.ep(k)
        remote(final.at[s], ret.at[s], a0.at[s], a1.at[s], s, p.t).wait_recv()
        final_copy(k).wait_send()
    head_move.wait_sent()


def outward(slots, message, gates, n_ep, n_tp):
    _, capacity, width = slots.shape
    sems = [DMA((n_ep,))] * 6 + spread_sems(n_ep, n_tp)
    return pl.pallas_call(
        functools.partial(outward_kernel, n_ep, n_tp),
        out_shape=[
            jax.ShapeDtypeStruct((n_ep, capacity, width * n_tp), slots.dtype),
            jax.ShapeDtypeStruct(message.shape, message.dtype),
            jax.ShapeDtypeStruct(gates.shape, gates.dtype),
        ],
        in_specs=[VM] * 3,
        out_specs=[VM] * 3,
        scratch_shapes=sems,
        compiler_params=pltpu.CompilerParams(collective_id=0, has_side_effects=True),
        name="outward",
    )(slots, message, gates)


def homeward(partial, heads, n_ep, n_tp):
    _, capacity, features = partial.shape
    width, ny = features // n_tp, n_tp // 2
    far = max(ny - 1, 1)
    scratch = [
        pltpu.VMEM((n_ep, ny, capacity, width), jnp.bfloat16),
        pltpu.VMEM((n_ep, capacity, width), jnp.float32),
        pltpu.VMEM((n_ep, far, capacity, width), jnp.bfloat16),
        pltpu.VMEM((n_ep, far, capacity, width), jnp.bfloat16),
        pltpu.VMEM((n_ep, capacity, width), jnp.bfloat16),
    ]
    sems = [DMA((n_ep,))] * 4 + [DMA((n_ep, ny))] * 2 + [DMA((n_ep, far))] * 2
    return pl.pallas_call(
        functools.partial(homeward_kernel, n_ep, n_tp),
        out_shape=[
            jax.ShapeDtypeStruct((n_ep, capacity, width), jnp.bfloat16),
            jax.ShapeDtypeStruct((n_tp,) + heads.shape, jnp.bfloat16),
        ],
        in_specs=[VM] * 2,
        out_specs=[VM] * 2,
        scratch_shapes=scratch + sems + spread_sems(n_ep, n_tp),
        compiler_params=pltpu.CompilerParams(collective_id=1, has_side_effects=True),
        name="homeward",
    )(partial, heads)


def on_device(
    mixer_tokens,
    mixer_gain,
    query_weight,
    key_weight,
    value_weight,
    forget_weight,
    forget_bias,
    output_weight,
    expert_tokens,
    expert_gain,
    routes,
    route_weights,
    gate_weight,
    up_weight,
    down_weight,
):
    n_ep, n_tp = lax.axis_size("ep"), lax.axis_size("tp")
    rows, features = mixer_tokens.shape
    local_heads = forget_weight.shape[1]
    share = n_ep // local_heads
    part = rows // share
    width = features // n_tp
    bf16, f32 = jnp.bfloat16, jnp.float32

    expert_normed = normed_rows(expert_tokens, expert_gain)
    token_count, top_count = routes.shape
    capacity = 2 * top_count * token_count // n_ep
    pairs = token_count * top_count
    flat_routes = routes.reshape(-1)
    onehot = flat_routes[:, None] == jnp.arange(n_ep, dtype=jnp.int32)[None, :]
    before = jnp.tril(jnp.ones((pairs, pairs), bf16), -1)
    ranks = jnp.dot(before, onehot.astype(bf16), preferred_element_type=f32)
    slot_rank = jnp.sum(jnp.where(onehot, ranks, 0.0), axis=1).astype(jnp.int32)
    slot_index = (flat_routes * capacity + slot_rank).reshape(token_count, top_count)
    slot_ids = jnp.arange(n_ep * capacity, dtype=jnp.int32)
    picks = [(slot_index[:, j][:, None] == slot_ids[None, :]).astype(bf16) for j in range(top_count)]
    column = lax.axis_index("tp") * width
    own_columns = lax.dynamic_slice_in_dim(expert_normed, column, width, 1)
    slots = lax.dot_general(
        sum(picks[1:], picks[0]), own_columns, (((0,), (0,)), ((), ())),
        preferred_element_type=f32,
    ).astype(bf16).reshape(n_ep, capacity, width)

    normed = normed_rows(mixer_tokens, mixer_gain)
    queries = by_rows(normed, query_weight).astype(bf16)
    key_rows = by_rows(normed, key_weight).astype(bf16)
    value_rows = by_rows(normed, value_weight).astype(bf16)
    pre_gate = jnp.dot(normed, forget_weight, preferred_element_type=f32) + forget_bias
    block_cum = jnp.dot(
        jnp.tril(jnp.ones((rows, rows), f32)), jax.nn.log_sigmoid(pre_gate),
        precision=lax.Precision.HIGHEST, preferred_element_type=f32,
    )
    key_value = jnp.concatenate(
        [
            key_rows.reshape(rows, local_heads, HD).transpose(1, 0, 2),
            value_rows.reshape(rows, local_heads, HD).transpose(1, 0, 2),
        ],
        axis=2,
    )
    key_value = jnp.broadcast_to(
        key_value[:, None], (local_heads, share, rows, 2 * HD)
    ).reshape(n_ep, rows, 2 * HD)
    half = part // 2
    query_parts = queries.reshape(share, 2, half, local_heads, HD).transpose(3, 0, 2, 1, 4)
    query_parts = query_parts.reshape(n_ep, half, 2 * HD)
    message = jnp.concatenate([key_value, query_parts], axis=1)
    gates = jnp.broadcast_to(block_cum.T[:, None, None, :], (local_heads, share, 1, rows))
    gates = gates.reshape(n_ep, 1, rows)

    all_slots, all_messages, all_gates = outward(slots, message, gates, n_ep, n_tp)

    positions = n_ep * rows
    all_gates = all_gates.reshape(n_ep, rows)
    totals = all_gates[:, rows - 1]
    lower = jnp.arange(n_ep)[None, :] < jnp.arange(n_ep)[:, None]
    base = jnp.sum(jnp.where(lower, totals[None, :], 0.0), axis=1)
    cumulative = all_gates + base[:, None]
    keys = all_messages[:, :rows, :HD].reshape(positions, HD)
    values = all_messages[:, :rows, HD:].reshape(positions, HD)
    head_query = all_messages[:, rows:].reshape(n_ep, half, 2, HD).transpose(0, 2, 1, 3)
    head_query = head_query.reshape(n_ep * part, HD)
    first = (lax.axis_index("ep") % share) * part
    query_cum = lax.dynamic_slice_in_dim(cumulative, first, part, 1).reshape(-1)
    query_pos = (
        jnp.arange(n_ep, dtype=jnp.int32)[:, None] * rows
        + first
        + jnp.arange(part, dtype=jnp.int32)[None, :]
    ).reshape(-1)
    key_pos = jnp.arange(positions, dtype=jnp.int32)
    scores = by_rows(head_query, keys) * HD ** (-0.5)
    scores = scores + query_cum[:, None] - cumulative.reshape(-1)[None, :]
    scores = jnp.where(key_pos[None, :] <= query_pos[:, None], scores, -jnp.inf)
    weights = jnp.exp(scores - jnp.max(scores, axis=-1, keepdims=True)).astype(bf16)
    attended = jnp.dot(weights, values, preferred_element_type=f32)
    rescale = lax.rsqrt(jnp.mean(attended * attended, axis=-1, keepdims=True) + HEAD_FLOOR)
    head_out = (attended * rescale).astype(bf16).reshape(n_ep, part, HD)

    flat_rows = all_slots.reshape(n_ep * capacity, features)
    gate_act = by_rows(flat_rows, gate_weight[0])
    up_act = by_rows(flat_rows, up_weight[0])
    hidden = (jax.nn.silu(gate_act) * up_act).astype(bf16)
    partial = jnp.dot(hidden, down_weight[0], preferred_element_type=f32).astype(bf16)
    partial = partial.reshape(n_ep, capacity, features)

    returned, heads_all = homeward(partial, head_out, n_ep, n_tp)

    heads_all = heads_all.reshape(n_tp, local_heads, share, part, HD).transpose(2, 3, 0, 1, 4)
    heads_all = heads_all.reshape(rows, n_tp * local_heads * HD)
    mixer_output = jnp.dot(heads_all, output_weight, preferred_element_type=f32).astype(bf16)
    returned = returned.reshape(n_ep * capacity, width)
    expert_output = 0.0
    for j in range(top_count):
        picked = jnp.dot(picks[j], returned, preferred_element_type=f32)
        expert_output = expert_output + picked * route_weights[:, j][:, None]
    return (mixer_output, expert_output.astype(bf16))


def solution(mesh):
    in_specs = (
        P("ep", None),
        P(),
        P("tp", None),
        P("tp", None),
        P("tp", None),
        P(None, "tp"),
        P("ep", "tp"),
        P(None, "tp"),
        P("ep", None),
        P(),
        P("ep", None),
        P("ep", None),
        P("ep", "tp", None),
        P("ep", "tp", None),
        P("ep", "tp", None),
    )
    out_specs = (P("ep", "tp"), P("ep", "tp"))
    return jax.shard_map(
        on_device, mesh=mesh, in_specs=in_specs, out_specs=out_specs, check_vma=False
    )
```

time: 208 us -> 104 us (0.50)
  blocking collectives: 123 us -> 0 us
  Pallas kernels: 0 us -> 64.7 us
  waiting for transfers between devices: 21.7 us -> 0 us
  between operations: 14.3 us -> 0.99 us
  starting transfers between devices: 6.33 us -> 0 us
  local copies, waits for them, and re-layouts: 12.8 us -> 6.94 us
  matrix products: 22.2 us -> 27.5 us
  other arithmetic: 7.21 us -> 3.95 us
    all_gather x4 -> x0, blocking collectives: 101 us -> none  [the longest x1 32.1 us: on_device(): lax.all_gather(key_rows, 'ep', axis=0, tiled=True)]
    pallas_call x0 -> x2, Pallas kernels: none -> 64.7 us  [the longest x1 35 us: homeward(): pl.pallas_call(functools.partial(homeward_kernel, n_ep, n_tp), out_shape=...]
    all_to_all x1 -> x0, blocking collectives: 21.7 us -> none  [on_device(): lax.all_to_all(slices, 'ep', split_axis=0, concat_axis=0, tiled=True)]
    all_gather x1 -> x0, waiting for transfers between devices: 21.7 us -> none  [on_device(): lax.all_gather(lax.all_to_all(slices, 'ep', split_axis=0, concat_axis=0,...]
    all_to_all x1 -> x0, starting transfers between devices: 6.25 us -> none  [on_device(): lax.all_to_all(summed, 'ep', split_axis=0, concat_axis=0, tiled=True)]
    gather x2 -> x0, local copies, waits for them, and re-layouts: 4.5 us -> none  [the longest x1 3.35 us: on_device(): outgoing = padded[slot_owner].reshape(experts, capacity, feature_count)]
    reshape x1 -> x9, local copies, waits for them, and re-layouts: 0.02 us -> 3.06 us  [the longest x1 1.46 us: on_device(): heads_all.reshape(n_tp, local_heads, share, part, HD)]
    dot_general x5, matrix products: 9.14 us -> 12 us  [by_rows(): lax.dot_general(left, weight, (((1,), (1,)), ((), ())), preferred_element...]
  transfers between devices with their start and end apart: 3 -> 0, of which waited for: 1 -> 0; matrix products, arithmetic and copies ran while one was open for 7% -> 0% of each run, Pallas kernels for 0% -> 0%
where the time goes in v1:
time: 104 us
  Pallas kernels  64.7 us (62%)
  matrix products  27.5 us (26%)
  local copies, waits for them, and re-layouts  6.94 us (7%)
  other arithmetic  3.95 us (4%)
    pallas_call x1, Pallas kernels, homeward(): pl.pallas_call(functools.partial(homeward_kernel, n_ep, n_tp), out_shape=...  35 us
    pallas_call x1, Pallas kernels, outward(): pl.pallas_call(functools.partial(outward_kernel, n_ep, n_tp), out_shape=[...  29.7 us
    dot_general x5, matrix products, by_rows(): lax.dot_general(left, weight, (((1,), (1,)), ((), ())), preferred_element...  12 us
    dot_general x1, matrix products, on_device(): jnp.dot(hidden, down_weight[0], preferred_element_type=f32).astype(bf16)  10.2 us

profile of v1, /device:TPU:0, one launch (start us, length us, event | category | flops | bytes accessed | tf_op | source)
XLA Modules:
  0.0 104.1 jit_solution(2753548112795150816)
XLA Ops:
  0.7 1.3 %convert_element_type.60 = f32[128,2048]{1,0:T(8,128)S(1)} convert(bf16[128,2048]{1,0:T(8,128)(2,1)} %param.23) | non-fusion elementwise | flops 262144 | bytes 1572864 | tf_op jit(solution)/shard_map/convert_element_type | solution.py:19
  2.0 0.8 dynamic-slice
  2.7 1.2 %multiply_reduce_fusion = f32[128]{0:T(128)S(1)} fusion(bf16[128,2048]{1,0:T(8,128)(2,1)} %param.23), kind=kLoop, calls=%fused_computation.31 | loop fusion | flops 786304 | bytes 524800 | tf_op jit(solution)/shard_map/reduce_sum | solution.py:20
  4.2 0.3 fusion.18
  4.7 1.2 %convolution_convert_fusion = bf16[512,512]{1,0:T(8,128)(2,1)} fusion(f32[128,2048]{1,0:T(8,128)S(1)} %convert_element_type.60, s32[]{:T(128)S(6)} %select_n.40, f32[512]{0:T(512)S(1)} %dynamic-slice, f32[128]{0:T(128)S(1)} %maximum_rsqrt_fusion.1, s32[128]{0:T(128)S(1)} %get-tuple-element.17, s32[128]{0:T(128)S(1)} %get-tuple-element.16), kind=kOutput, calls=%fused_computation.18 | convolution fusion | flops 68091904 | bytes 790020 | tf_op jit(solution)/shard_map/dot_general | solution.py:360
  6.2 1.8 %convolution_convert_fusion.2 = bf16[192,256]{1,0:T(8,128)(2,1)S(1)} fusion(bf16[256,2048]{1,0:T(8,128)(2,1)} %param.17, bf16[192,2048]{1,0:T(8,128)(2,1)S(1)} %copy-done.3, f32[2048]{0:T(1024)S(1)} %copy-done.9, f32[192]{0:T(256)S(1)} %maximum_rsqrt_fusion), kind=kOutput, calls=%fused_computation.24 | convolution fusion | flops 202948608 | bytes 1942272 | tf_op jit(solution)/shard_map/dot_general | solution.py:25
  8.5 0.5 convolution_convert_fusion.3
  9.2 1.7 %convolution_convert_fusion.4 = bf16[192,256]{1,0:T(8,128)(2,1)S(1)} fusion(bf16[256,2048]{1,0:T(8,128)(2,1)} %param.18, bf16[192,2048]{1,0:T(8,128)(2,1)S(1)} %copy-done.3, f32[2048]{0:T(1024)S(1)} %copy-done.9, f32[192]{0:T(256)S(1)} %maximum_rsqrt_fusion), kind=kOutput, calls=%fused_computation.26 | convolution fusion | flops 202948608 | bytes 1942272 | tf_op jit(solution)/shard_map/dot_general | solution.py:25
  11.3 0.8 pad_maximum_fusion.message
  12.2 0.4 fusion.19
  12.8 0.6 broadcast_in_dim.72.gates
  13.5 29.7 %outward.1 = (bf16[8,64,2048]{2,1,0:T(8,128)(2,1)}, bf16[8,240,128]{2,1,0:T(8,128)(2,1)}, f32[8,1,192]{2,1,0:T(1,128)}) custom-call(bf16[8,64,512]{2,1,0:T(8,128)(2,1)} %bitcast.65, bf16[8,240,128]{2,1,0:T(8,128)(2,1)} %pad_maximum_fusion.message, f32[8,1,192]{2,1,0:T(1,128)} %broadcast_in_dim.72.gates), custom_call_target="tpu_custom_call" | custom-call | tf_op jit(solution)/shard_map/outward/pallas_call | solution.py:280
  43.2 6.3 %fusion.4 = f32[512,896]{1,0:T(8,128)} fusion(bf16[512,2048]{1,0:T(8,128)(2,1)} %bitcast.80, bf16[1,896,2048]{2,1,0:T(8,128)(2,1)} %param.27), kind=kOutput, calls=%fused_computation.7 | convolution fusion | flops 1879048192 | bytes 7602176 | tf_op jit(solution)/shard_map/dot_general | solution.py:25
  49.5 10.2 %fusion.6 = bf16[512,2048]{1,0:T(8,128)(2,1)} fusion(bf16[1,896,2048]{2,1,0:T(8,128)(2,1)} %param.29, f32[512,896]{1,0:T(8,128)} %fusion.4, bf16[512,2048]{1,0:T(8,128)(2,1)} %bitcast.81, bf16[1,896,2048]{2,1,0:T(8,128)(2,1)} %param.28), kind=kOutput, calls=%fused_computation.9 | convolution fusion | flops 3761897472 | bytes 13369344 | tf_op jit(solution)/shard_map/dot_general | solution.py:423
  60.7 0.4 copy.56
  61.5 1.6 %fusion.66 = (f32[768]{0:T(1024)S(1)}, f32[768,1536]{1,0:T(8,128)S(1)}) fusion(f32[1536]{0:T(1024)S(1)} %add.140, f32[768]{0:T(1024)S(1)} %add.136, bf16[768,64]{0,1:T(8,128)(2,1)S(1)} %reshape.141, bf16[1536,64]{1,0:T(8,128)(2,1)S(1)} %bitcast.77, s32[768]{0:T(1024)S(1)} %add.132), kind=kOutput, calls=%fused_computation.95 | convolution fusion | flops 158072064 | bytes 5028864 | tf_op jit(solution)/shard_map/dot_general | solution.py:25
  63.1 1.0 multiply_reduce_fusion.1
  64.1 0.8 copy.57
  64.9 35.0 %homeward.1 = (bf16[8,64,512]{2,1,0:T(8,128)(2,1)}, bf16[4,8,96,64]{3,2,1,0:T(8,128)(2,1)}) custom-call(bf16[8,64,2048]{2,1,0:T(8,128)(2,1)} %bitcast.64, bf16[8,96,64]{2,1,0:T(8,128)(2,1)} %bitcast.72), custom_call_target="tpu_custom_call" | custom-call | tf_op jit(solution)/shard_map/homeward/pallas_call | solution.py:307
  100.0 1.5 %copy.58 = bf16[4,4,2,96,64]{3,2,4,1,0:T(2,128)(2,1)S(1)} copy(bf16[4,4,2,96,64]{4,3,2,1,0:T(8,128)(2,1)} %bitcast.73) | data formatting | bytes 786432 | tf_op jit(solution)/shard_map/reshape | solution.py:428
  101.5 0.3 reshape.148
  101.8 1.1 %convolution_convert_fusion.1 = bf16[192,512]{1,0:T(8,128)(2,1)} fusion(bf16[192,1024]{0,1:T(8,128)(2,1)S(1)} %reshape.148, bf16[1024,512]{1,0:T(8,128)(2,1)S(1)} %copy-done), kind=kOutput, calls=%fused_computation.19 | convolution fusion | flops 201424896 | bytes 1638400 | tf_op jit(solution)/shard_map/dot_general | solution.py:430
  102.9 0.3 convolution_multiply_fusion.1
  103.2 0.9 fusion.17
  (63 shorter events, 3.4 us)
Async XLA Ops:
  0.6 101.2 %copy-start = (bf16[1024,512]{1,0:T(8,128)(2,1)S(1)}, bf16[1024,512]{1,0:T(8,128)(2,1)}, u32[]{:S(2)}) copy-start(bf16[1024,512]{1,0:T(8,128)(2,1)} %param.22) | copy-start | bytes 3145732
  0.6 3.3 %copy-start.5 = (s32[128,2]{0,1:T(2,128)S(1)}, s32[128,2]{0,1:T(2,128)}, u32[]{:S(2)}) copy-start(s32[128,2]{0,1:T(2,128)} %param.25) | copy-start | bytes 3076
  0.7 5.3 %copy-start.3 = (bf16[192,2048]{1,0:T(8,128)(2,1)S(1)}, bf16[192,2048]{1,0:T(8,128)(2,1)}, u32[]{:S(2)}) copy-start(bf16[192,2048]{1,0:T(8,128)(2,1)} %param.15) | copy-start | bytes 2359300
  0.7 5.6 %copy-start.9 = (f32[2048]{0:T(1024)S(1)}, f32[2048]{0:T(1024)}, u32[]{:S(2)}) copy-start(f32[2048]{0:T(1024)} %param.16) | copy-start | bytes 24580
  6.0 2.6 %copy-start.7 = (bf16[256,2048]{1,0:T(8,128)(2,1)S(1)}, bf16[256,2048]{1,0:T(8,128)(2,1)}, u32[]{:S(2)}) copy-start(bf16[256,2048]{1,0:T(8,128)(2,1)} %param.19) | copy-start | bytes 3145732
  9.2 3.0 %copy-start.8 = (bf16[2048,4]{0,1:T(4,128)(2,1)S(1)}, bf16[2048,4]{0,1:T(4,128)(2,1)}, u32[]{:S(2)}) copy-start(bf16[2048,4]{0,1:T(4,128)(2,1)} %param.20) | copy-start | bytes 49156
  9.2 3.0 %copy-start.10 = (f32[1,4]{1,0:T(1,128)S(1)}, f32[1,4]{1,0:T(1,128)}, u32[]{:S(2)}) copy-start(f32[1,4]{1,0:T(1,128)} %param.21) | copy-start | bytes 52
  49.5 10.2 %copy-start.2 = (bf16[8,240,128]{2,1,0:T(8,128)(2,1)S(1)}, bf16[8,240,128]{2,1,0:T(8,128)(2,1)}, u32[]{:S(2)}) copy-start(bf16[8,240,128]{2,1,0:T(8,128)(2,1)} %get-tuple-element.8) | copy-start | bytes 1474564
  49.5 10.4 %copy-start.4 = (f32[8,1,192]{2,1,0:T(1,128)S(1)}, f32[8,1,192]{2,1,0:T(1,128)}, u32[]{:S(2)}) copy-start(f32[8,1,192]{2,1,0:T(1,128)} %get-tuple-element.9) | copy-start | bytes 18436
  100.0 2.9 %copy-start.6 = (f32[128,2]{0,1:T(2,128)S(1)}, f32[128,2]{0,1:T(2,128)}, u32[]{:S(2)}) copy-start(f32[128,2]{0,1:T(2,128)} %param.26) | copy-start | bytes 3076
  100.0 2.9 %copy-start.1 = (bf16[8,64,512]{2,1,0:T(8,128)(2,1)S(1)}, bf16[8,64,512]{2,1,0:T(8,128)(2,1)}, u32[]{:S(2)}) copy-start(bf16[8,64,512]{2,1,0:T(8,128)(2,1)} %get-tuple-element.11) | copy-start | bytes 1572868

commit v2 on v1

--- a/solution.py
+++ b/solution.py
@@ -12,6 +12,7 @@
 HEAD_FLOOR = 1.0
 MESH = pl.DeviceIdType.MESH
 VM = pl.BlockSpec(memory_space=pltpu.VMEM)
+ANY = pl.BlockSpec(memory_space=pl.ANY)
 DMA = pltpu.SemaphoreType.DMA
 
 
@@ -150,6 +151,10 @@
     def finish(self, s):
         for off in range(self.p.ny):
             self.p_arrival(off, s).wait_recv()
+        self.wait_sent(s)
+
+    def wait_sent(self, s):
+        for off in range(self.p.ny):
             self.p_copy(off, s).wait_send()
         for off in range(1, self.p.ny):
             self.y_copy(off, s).wait_send()
@@ -162,15 +167,32 @@
 
 
 def outward_kernel(
-    n_ep, n_tp, slots, message, gates, out, message_out, gates_out,
-    s0, s1, m0, m1, g0, g1, ys, yr, ps, pr,
+    n_ep, n_tp, slots, message, gates, gate_weight, up_weight,
+    hidden, message_out, gates_out,
+    out, gate_held, up_held, gate_act, up_act,
+    s0, s1, m0, m1, g0, g1, w, ys, yr, ps, pr,
 ):
     p = Place(n_ep, n_tp)
     width = slots.shape[2]
 
+    def cols(t):
+        return pl.ds(pl.multiple_of(t * width, width), width)
+
     def land(t, s):
-        return out.at[s, :, pl.ds(pl.multiple_of(t * width, width), width)]
-
+        return out.at[s, :, cols(t)]
+
+    def multiply(t, opening):
+        rows = out[:, :, cols(t)].reshape(hidden.shape[0], width)
+        for held, total in ((gate_held, gate_act), (up_held, up_act)):
+            product = by_rows(rows, held[:, cols(t)])
+            total[...] = product if opening else total[...] + product
+
+    loads = [
+        pltpu.make_async_copy(gate_weight, gate_held, w.at[0]),
+        pltpu.make_async_copy(up_weight, up_held, w.at[1]),
+    ]
+    for load in loads:
+        load.start()
     p.barrier()
     slot_move = Exchange(p, lambda d: slots.at[d], lambda s: land(p.t, s), (s0, s1))
     gate_move = Exchange(p, lambda d: gates.at[d], lambda s: gates_out.at[s], (g0, g1))
@@ -182,21 +204,34 @@
     for k in range(n_ep):
         slot_move.wait_arrival(k)
         spread.first(p.ep(k))
+    for load in loads:
+        load.wait()
+    multiply(p.t, True)
+    for k in range(n_ep):
+        spread.p_arrival(0, p.ep(k)).wait_recv()
+    multiply(p.partner, False)
     for k in range(n_ep):
         spread.relay(p.ep(k))
+    for off in range(1, p.ny):
+        multiply(p.chip(-off), False)
+        for k in range(n_ep):
+            spread.p_arrival(off, p.ep(k)).wait_recv()
+        multiply(p.y_at(-off) * 2 + (1 - p.c), False)
+    gate = gate_act[...]
+    hidden[...] = (gate * lax.logistic(gate) * up_act[...]).astype(hidden.dtype)
     for k in range(n_ep):
         gate_move.wait_arrival(k)
         message_move.wait_arrival(k)
-        spread.finish(p.ep(k))
+        spread.wait_sent(p.ep(k))
     slot_move.wait_sent()
     gate_move.wait_sent()
     message_move.wait_sent()
 
 
 def homeward_kernel(
-    n_ep, n_tp, partial, heads, ret, heads_all,
-    pair, mine, out_y, in_y, final,
-    h0, h1, a0, a1, r0, r1, q0, q1, ys, yr, ps, pr,
+    n_ep, n_tp, hidden, down_weight, heads, ret, heads_all,
+    partial, down_held, pair, mine, out_y, in_y, final,
+    w, h0, h1, a0, a1, r0, r1, q0, q1, ys, yr, ps, pr,
 ):
     p = Place(n_ep, n_tp)
     ny = p.ny
@@ -208,6 +243,8 @@
     def land(t, s):
         return heads_all.at[t, s]
 
+    load = pltpu.make_async_copy(down_weight, down_held, w.at[0])
+    load.start()
     p.barrier()
     head_move = Exchange(p, lambda d: heads.at[d], lambda s: land(p.t, s), (h0, h1))
     spread = Spread(p, land, (ys, yr, ps, pr))
@@ -228,12 +265,23 @@
         return remote(final.at[d], ret.at[p.e], a0.at[d], a1.at[p.e], d, p.t)
 
     order = list(range(1, n_ep)) + [0]
-    for k in order:
-        for off in range(ny):
+    capacity = ret.shape[1]
+
+    def multiply(t):
+        product = jnp.dot(
+            hidden[...], down_held[:, cols(t)], preferred_element_type=jnp.float32
+        )
+        partial[:, :, cols(t)] = product.astype(jnp.bfloat16).reshape(n_ep, capacity, width)
+
+    load.wait()
+    turns = [*range(1, ny), 0]
+    for off in turns:
+        multiply(p.y_at(off) * 2 + (1 - p.c))
+        multiply(p.chip(off))
+        for k in order:
             pair_copy(p.ep(k), off).start()
-    for k in order:
-        s = p.ep(k)
-        for off in [*range(1, ny), 0]:
+        for k in order:
+            s = p.ep(k)
             pair_copy(s, off).wait_recv()
             both = partial[s, :, cols(p.chip(off))].astype(jnp.float32) + pair[s, off].astype(
                 jnp.float32
@@ -274,48 +322,58 @@
     head_move.wait_sent()
 
 
-def outward(slots, message, gates, n_ep, n_tp):
+def outward(slots, message, gates, gate_weight, up_weight, n_ep, n_tp):
     _, capacity, width = slots.shape
-    sems = [DMA((n_ep,))] * 6 + spread_sems(n_ep, n_tp)
+    rows, units = n_ep * capacity, gate_weight.shape[0]
+    scratch = [
+        pltpu.VMEM((n_ep, capacity, width * n_tp), slots.dtype),
+        pltpu.VMEM(gate_weight.shape, gate_weight.dtype),
+        pltpu.VMEM(up_weight.shape, up_weight.dtype),
+        pltpu.VMEM((rows, units), jnp.float32),
+        pltpu.VMEM((rows, units), jnp.float32),
+    ]
+    sems = [DMA((n_ep,))] * 6 + [DMA((2,))] + spread_sems(n_ep, n_tp)
     return pl.pallas_call(
         functools.partial(outward_kernel, n_ep, n_tp),
         out_shape=[
-            jax.ShapeDtypeStruct((n_ep, capacity, width * n_tp), slots.dtype),
+            jax.ShapeDtypeStruct((rows, units), slots.dtype),
             jax.ShapeDtypeStruct(message.shape, message.dtype),
             jax.ShapeDtypeStruct(gates.shape, gates.dtype),
         ],
-        in_specs=[VM] * 3,
+        in_specs=[VM] * 3 + [ANY] * 2,
         out_specs=[VM] * 3,
-        scratch_shapes=sems,
+        scratch_shapes=scratch + sems,
         compiler_params=pltpu.CompilerParams(collective_id=0, has_side_effects=True),
         name="outward",
-    )(slots, message, gates)
-
-
-def homeward(partial, heads, n_ep, n_tp):
-    _, capacity, features = partial.shape
+    )(slots, message, gates, gate_weight, up_weight)
+
+
+def homeward(hidden, down_weight, heads, n_ep, n_tp):
+    capacity, features = hidden.shape[0] // n_ep, down_weight.shape[1]
     width, ny = features // n_tp, n_tp // 2
     far = max(ny - 1, 1)
     scratch = [
+        pltpu.VMEM((n_ep, capacity, features), jnp.bfloat16),
+        pltpu.VMEM(down_weight.shape, down_weight.dtype),
         pltpu.VMEM((n_ep, ny, capacity, width), jnp.bfloat16),
         pltpu.VMEM((n_ep, capacity, width), jnp.float32),
         pltpu.VMEM((n_ep, far, capacity, width), jnp.bfloat16),
         pltpu.VMEM((n_ep, far, capacity, width), jnp.bfloat16),
         pltpu.VMEM((n_ep, capacity, width), jnp.bfloat16),
     ]
-    sems = [DMA((n_ep,))] * 4 + [DMA((n_ep, ny))] * 2 + [DMA((n_ep, far))] * 2
+    sems = [DMA((1,))] + [DMA((n_ep,))] * 4 + [DMA((n_ep, ny))] * 2 + [DMA((n_ep, far))] * 2
     return pl.pallas_call(
         functools.partial(homeward_kernel, n_ep, n_tp),
         out_shape=[
             jax.ShapeDtypeStruct((n_ep, capacity, width), jnp.bfloat16),
             jax.ShapeDtypeStruct((n_tp,) + heads.shape, jnp.bfloat16),
         ],
-        in_specs=[VM] * 2,
+        in_specs=[VM, ANY, VM],
         out_specs=[VM] * 2,
         scratch_shapes=scratch + sems + spread_sems(n_ep, n_tp),
         compiler_params=pltpu.CompilerParams(collective_id=1, has_side_effects=True),
         name="homeward",
-    )(partial, heads)
+    )(hidden, down_weight, heads)
 
 
 def on_device(
@@ -388,7 +446,9 @@
     gates = jnp.broadcast_to(block_cum.T[:, None, None, :], (local_heads, share, 1, rows))
     gates = gates.reshape(n_ep, 1, rows)
 
-    all_slots, all_messages, all_gates = outward(slots, message, gates, n_ep, n_tp)
+    hidden, all_messages, all_gates = outward(
+        slots, message, gates, gate_weight[0], up_weight[0], n_ep, n_tp
+    )
 
     positions = n_ep * rows
     all_gates = all_gates.reshape(n_ep, rows)
@@ -416,14 +476,7 @@
     rescale = lax.rsqrt(jnp.mean(attended * attended, axis=-1, keepdims=True) + HEAD_FLOOR)
     head_out = (attended * rescale).astype(bf16).reshape(n_ep, part, HD)
 
-    flat_rows = all_slots.reshape(n_ep * capacity, features)
-    gate_act = by_rows(flat_rows, gate_weight[0])
-    up_act = by_rows(flat_rows, up_weight[0])
-    hidden = (jax.nn.silu(gate_act) * up_act).astype(bf16)
-    partial = jnp.dot(hidden, down_weight[0], preferred_element_type=f32).astype(bf16)
-    partial = partial.reshape(n_ep, capacity, features)
-
-    returned, heads_all = homeward(partial, head_out, n_ep, n_tp)
+    returned, heads_all = homeward(hidden, down_weight[0], head_out, n_ep, n_tp)
 
     heads_all = heads_all.reshape(n_tp, local_heads, share, part, HD).transpose(2, 3, 0, 1, 4)
     heads_all = heads_all.reshape(rows, n_tp * local_heads * HD)

time: 104 us -> 89.8 us (0.86)
  matrix products: 27.5 us -> 9.7 us
  local copies, waits for them, and re-layouts: 6.94 us -> 9.12 us
  Pallas kernels: 64.7 us -> 66.7 us
    dot_general x1 -> x0, matrix products: 10.2 us -> none  [on_device(): jnp.dot(hidden, down_weight[0], preferred_element_type=f32).astype(bf16)]
    dot_general x5 -> x4, matrix products: 12 us -> 4.37 us  [by_rows(): lax.dot_general(left, weight, (((1,), (1,)), ((), ())), preferred_element...]
    pallas_call x1, Pallas kernels: 35 us -> 37.5 us  [homeward(): pl.pallas_call(functools.partial(homeward_kernel, n_ep, n_tp), out_shape=...]
    slice x1, local copies, waits for them, and re-layouts: 0.18 us -> 1.3 us  [on_device(): keys = all_messages[:, :rows, :HD].reshape(positions, HD)]
    reduce_sum x2, other arithmetic: 1.47 us -> 0.42 us  [normed_rows(): square = jnp.mean(values * values, axis=-1, keepdims=True)]
where the time goes in v2:
time: 89.8 us; the launch traced here: 89.5 us
  Pallas kernels  66.7 us (74%)
  matrix products  9.7 us (11%)
  local copies, waits for them, and re-layouts  9.12 us (10%)
  other arithmetic  2.92 us (3%)
  between operations  1.01 us (1%)
    pallas_call x1, Pallas kernels, homeward(): pl.pallas_call(functools.partial(homeward_kernel, n_ep, n_tp), out_shape=...  37.5 us
    pallas_call x1, Pallas kernels, outward(): pl.pallas_call(functools.partial(outward_kernel, n_ep, n_tp), out_shape=[...  29.3 us
    dot_general x4, matrix products, by_rows(): lax.dot_general(left, weight, (((1,), (1,)), ((), ())), preferred_element...  4.37 us

profile of v2, /device:TPU:0, one launch (start us, length us, event | category | flops | bytes accessed | tf_op | source)
XLA Modules:
  0.0 89.5 jit_solution(9875453447772114219)
XLA Ops:
  0.7 1.3 %convert_element_type.54 = f32[128,2048]{1,0:T(8,128)S(1)} convert(bf16[128,2048]{1,0:T(8,128)(2,1)} %param.23) | non-fusion elementwise | flops 262144 | bytes 1572864 | tf_op jit(solution)/shard_map/convert_element_type | solution.py:20
  2.0 0.8 dynamic-slice
  3.2 0.3 fusion.7
  3.7 1.2 %convolution_convert_fusion = bf16[512,512]{1,0:T(8,128)(2,1)} fusion(f32[128,2048]{1,0:T(8,128)S(1)} %convert_element_type.54, s32[]{:T(128)S(6)} %select_n.40, f32[512]{0:T(512)S(1)} %dynamic-slice, f32[128]{0:T(128)S(1)} %maximum_rsqrt_fusion.1, s32[128]{0:T(128)S(1)} %get-tuple-element.17, s32[128]{0:T(128)S(1)} %get-tuple-element.16), kind=kOutput, calls=%fused_computation.10 | convolution fusion | flops 68091904 | bytes 790020 | tf_op jit(solution)/shard_map/dot_general | solution.py:418
  5.2 0.5 convolution_convert_fusion.2
  6.5 0.5 convolution_convert_fusion.3
  7.1 1.7 %convolution_convert_fusion.4 = bf16[192,256]{1,0:T(8,128)(2,1)S(1)} fusion(bf16[256,2048]{1,0:T(8,128)(2,1)} %param.18, bf16[192,2048]{1,0:T(8,128)(2,1)S(1)} %copy-done.3, f32[2048]{0:T(1024)S(1)} %copy-done.10, f32[192]{0:T(256)S(1)} %maximum_rsqrt_fusion), kind=kOutput, calls=%fused_computation.18 | convolution fusion | flops 202948608 | bytes 1942272 | tf_op jit(solution)/shard_map/dot_general | solution.py:26
  9.2 0.8 pad_maximum_fusion.message
  10.1 0.4 fusion.8
  10.7 0.6 broadcast_in_dim.72.gates
  11.4 29.3 %outward.1 = (bf16[512,896]{1,0:T(8,128)(2,1)}, bf16[8,240,128]{2,1,0:T(8,128)(2,1)}, f32[8,1,192]{2,1,0:T(1,128)}) custom-call(bf16[8,64,512]{2,1,0:T(8,128)(2,1)} %bitcast.51, bf16[8,240,128]{2,1,0:T(8,128)(2,1)} %pad_maximum_fusion.message, f32[8,1,192]{2,1,0:T(1,128)} %broadcast_in_dim.72.gates, bf16[896,2048]{1,0:T(8,128)(2,1)} %bitcast.48, ...), custom_call_target="tpu_custom_call" | custom-call | tf_op jit(solution)/shard_map/outward/pallas_call | solution.py:336
  40.7 1.3 %fusion.51 = (bf16[8,192,64]{2,1,0:T(8,128)(2,1)S(1)}, bf16[8,192,64]{2,1,0:T(8,128)(2,1)S(1)}) fusion(bf16[8,240,128]{2,1,0:T(8,128)(2,1)} %get-tuple-element.8), kind=kLoop, calls=%fused_computation.85 | loop fusion | bytes 786432 | tf_op jit(solution)/shard_map/slice | solution.py:459
  42.7 0.9 %slice.26 = bf16[8,48,128]{2,1,0:T(8,128)(2,1)S(1)} slice(bf16[8,240,128]{2,1,0:T(8,128)(2,1)} %get-tuple-element.8), slice={[0:8], [192:240], [0:128]} | slice | bytes 196608 | tf_op jit(solution)/shard_map/slice | solution.py:461
  43.7 0.4 copy.56
  44.1 0.3 reshape.133
  44.5 1.6 %fusion.52 = (f32[768]{0:T(1024)S(1)}, f32[768,1536]{1,0:T(8,128)S(1)}) fusion(f32[1536]{0:T(1024)S(1)} %add.135, f32[768]{0:T(1024)S(1)} %add.131, bf16[768,64]{0,1:T(8,128)(2,1)S(1)} %reshape.133, bf16[1536,64]{1,0:T(8,128)(2,1)S(1)} %bitcast.63, s32[768]{0:T(1024)S(1)} %add.127), kind=kOutput, calls=%fused_computation.86 | convolution fusion | flops 158072064 | bytes 5028864 | tf_op jit(solution)/shard_map/dot_general | solution.py:26
  46.1 1.0 %multiply_reduce_fusion.1 = (f32[768]{0:T(1024)S(1)}, f32[768,64]{0,1:T(8,128)S(1)}) fusion(bf16[1536,64]{1,0:T(8,128)(2,1)S(1)} %bitcast.56, f32[768,1536]{1,0:T(8,128)S(1)} %get-tuple-element.19, f32[768]{0:T(1024)S(1)} %get-tuple-element.18), kind=kOutput, calls=%fused_computation.37 | convolution fusion | flops 153451776 | bytes 5117952 | tf_op jit(solution)/shard_map/dot_general | solution.py:475
  47.1 0.8 copy.57
  47.9 37.5 %homeward.1 = (bf16[8,64,512]{2,1,0:T(8,128)(2,1)}, bf16[4,8,96,64]{3,2,1,0:T(8,128)(2,1)}) custom-call(bf16[512,896]{1,0:T(8,128)(2,1)} %get-tuple-element.7.hidden, bf16[896,2048]{1,0:T(8,128)(2,1)} %bitcast.50, bf16[8,96,64]{2,1,0:T(8,128)(2,1)} %bitcast.58), custom_call_target="tpu_custom_call" | custom-call | tf_op jit(solution)/shard_map/homeward/pallas_call | solution.py:365
  85.4 1.4 %copy.58 = bf16[4,4,2,96,64]{3,2,4,1,0:T(2,128)(2,1)S(1)} copy(bf16[4,4,2,96,64]{4,3,2,1,0:T(8,128)(2,1)} %bitcast.59) | data formatting | bytes 786432 | tf_op jit(solution)/shard_map/reshape | solution.py:481
  86.8 0.3 reshape.140
  87.2 1.1 %convolution_convert_fusion.1 = bf16[192,512]{1,0:T(8,128)(2,1)} fusion(bf16[192,1024]{0,1:T(8,128)(2,1)S(1)} %reshape.140, bf16[1024,512]{1,0:T(8,128)(2,1)S(1)} %copy-done), kind=kOutput, calls=%fused_computation.11 | convolution fusion | flops 201424896 | bytes 1638400 | tf_op jit(solution)/shard_map/dot_general | solution.py:483
  88.3 0.3 convolution_multiply_fusion.1
  88.5 0.9 %fusion.6 = bf16[128,512]{1,0:T(8,128)(2,1)} fusion(f32[128,512]{1,0:T(8,128)S(1)} %convolution_multiply_fusion.1, bf16[512,512]{1,0:T(8,128)(2,1)S(1)} %bitcast.53, f32[128]{0:T(128)S(1)} %get-tuple-element.14, s32[128]{0:T(128)S(1)} %get-tuple-element.17), kind=kOutput, calls=%fused_computation.15 | convolution fusion | flops 67371008 | bytes 918528 | tf_op jit(solution)/shard_map/dot_general | solution.py:487
  (63 shorter events, 3.4 us)
Async XLA Ops:
  0.6 86.5 %copy-start = (bf16[1024,512]{1,0:T(8,128)(2,1)S(1)}, bf16[1024,512]{1,0:T(8,128)(2,1)}, u32[]{:S(2)}) copy-start(bf16[1024,512]{1,0:T(8,128)(2,1)} %param.22) | copy-start | bytes 3145732
  0.6 2.1 %copy-start.1 = (bf16[128,2048]{1,0:T(8,128)(2,1)S(1)}, bf16[128,2048]{1,0:T(8,128)(2,1)}, u32[]{:S(2)}) copy-start(bf16[128,2048]{1,0:T(8,128)(2,1)} %param.23) | copy-start | bytes 1572868
  0.7 2.3 %copy-start.5 = (s32[128,2]{0,1:T(2,128)S(1)}, s32[128,2]{0,1:T(2,128)}, u32[]{:S(2)}) copy-start(s32[128,2]{0,1:T(2,128)} %param.25) | copy-start | bytes 3076
  0.7 4.3 %copy-start.3 = (bf16[192,2048]{1,0:T(8,128)(2,1)S(1)}, bf16[192,2048]{1,0:T(8,128)(2,1)}, u32[]{:S(2)}) copy-start(bf16[192,2048]{1,0:T(8,128)(2,1)} %param.15) | copy-start | bytes 2359300
  2.0 3.2 %copy-start.10 = (f32[2048]{0:T(1024)S(1)}, f32[2048]{0:T(1024)}, u32[]{:S(2)}) copy-start(f32[2048]{0:T(1024)} %param.16) | copy-start | bytes 24580
  3.7 1.5 %copy-start.7 = (bf16[256,2048]{1,0:T(8,128)(2,1)S(1)}, bf16[256,2048]{1,0:T(8,128)(2,1)}, u32[]{:S(2)}) copy-start(bf16[256,2048]{1,0:T(8,128)(2,1)} %param.17) | copy-start | bytes 3145732
  5.2 1.2 %copy-start.8 = (bf16[256,2048]{1,0:T(8,128)(2,1)S(1)}, bf16[256,2048]{1,0:T(8,128)(2,1)}, u32[]{:S(2)}) copy-start(bf16[256,2048]{1,0:T(8,128)(2,1)} %param.19) | copy-start | bytes 3145732
  8.8 1.2 %copy-start.9 = (bf16[2048,4]{0,1:T(4,128)(2,1)S(1)}, bf16[2048,4]{0,1:T(4,128)(2,1)}, u32[]{:S(2)}) copy-start(bf16[2048,4]{0,1:T(4,128)(2,1)} %param.20) | copy-start | bytes 49156
  8.8 1.2 %copy-start.11 = (f32[1,4]{1,0:T(1,128)S(1)}, f32[1,4]{1,0:T(1,128)}, u32[]{:S(2)}) copy-start(f32[1,4]{1,0:T(1,128)} %param.21) | copy-start | bytes 52
  40.7 1.3 %copy-start.4 = (f32[8,1,192]{2,1,0:T(1,128)S(1)}, f32[8,1,192]{2,1,0:T(1,128)}, u32[]{:S(2)}) copy-start(f32[8,1,192]{2,1,0:T(1,128)} %get-tuple-element.9) | copy-start | bytes 18436
  86.8 1.4 %copy-start.6 = (f32[128,2]{0,1:T(2,128)S(1)}, f32[128,2]{0,1:T(2,128)}, u32[]{:S(2)}) copy-start(f32[128,2]{0,1:T(2,128)} %param.26) | copy-start | bytes 3076
  86.8 1.4 %copy-start.2 = (bf16[8,64,512]{2,1,0:T(8,128)(2,1)S(1)}, bf16[8,64,512]{2,1,0:T(8,128)(2,1)}, u32[]{:S(2)}) copy-start(bf16[8,64,512]{2,1,0:T(8,128)(2,1)} %get-tuple-element.11) | copy-start | bytes 1572868
